TPU v7x, 32 devices: a whole 2x2x4 slice. The times are simulated.
32 devices in a mesh: ep: 16 (over z, y, x), tp: 2 (over core).
Axes of the slice: x: 2, y: 2, z: 4, core: 2. Of those that a mesh axis runs over, the one named last changes fastest.
Arguments:
- tokens: bfloat16 [512, 2048], P('ep'), may hold values from -6 to 6
- lru_state: float32 [512, 1024], P('ep', 'tp'), may hold values from -6 to 6
- conv_window: bfloat16 [512, 3, 1024], P('ep', None, 'tp'), may hold values from -6 to 6
- gain_mix_in: float32 [2048], replicated, may hold values from 0.1 to 1.9
- gain_mix_out: float32 [2048], replicated, may hold values from 0.1 to 1.9
- gain_ffn_in: float32 [2048], replicated, may hold values from 0.1 to 1.9
- gain_ffn_out: float32 [2048], replicated, may hold values from 0.1 to 1.9
- w_branch: bfloat16 [2048, 1024], P(None, 'tp'), may hold values from -0.125 to 0.125
- w_input: bfloat16 [2048, 1024], P(None, 'tp'), may hold values from -0.125 to 0.125
- conv_taps: bfloat16 [4, 1024], P(None, 'tp'), may hold values from -3 to 3
- gate_a: bfloat16 [8, 128, 128], P('tp'), may hold values from -0.5 to 0.5
- gate_x: bfloat16 [8, 128, 128], P('tp'), may hold values from -0.5 to 0.5
- decay_rate: float32 [1024], P('tp'), may hold values from 0.001 to 0.3
- w_mix_out: bfloat16 [1024, 2048], P('tp'), may hold values from -0.1875 to 0.1875
- routes: int32 [512, 4], P('ep'), may hold values from 0 to 15, all different within a row; in each aligned block of 32 rows (0 to 31, 32 to 63, ...) at most 16 rows name the same one
- route_weight: float32 [512, 4], P('ep'), may hold values from 0.2 to 1.5
- expert_gate: bfloat16 [16, 2048, 512], P('ep', None, 'tp'), may hold values from -0.125 to 0.125
- expert_up: bfloat16 [16, 2048, 512], P('ep', None, 'tp'), may hold values from -0.125 to 0.125
- expert_down: bfloat16 [16, 512, 2048], P('ep', 'tp'), may hold values from -0.25 to 0.25
- shared_gate: bfloat16 [2048, 512], P(None, 'tp'), may hold values from -0.125 to 0.125
- shared_up: bfloat16 [2048, 512], P(None, 'tp'), may hold values from -0.125 to 0.125
- shared_down: bfloat16 [512, 2048], P('tp'), may hold values from -0.25 to 0.25
Outputs:
- layer_out: bfloat16 [512, 2048], P('ep')
- new_state: float32 [512, 1024], P('ep', 'tp')
- new_window: bfloat16 [512, 3, 1024], P('ep', None, 'tp')
Inputs may be any that keep to these rules, and one draw needn't show every extreme that they name: `routes`: each row names 4 different experts. Within the rows of one device (aligned blocks of 32 rows) no expert is named by more than 16 entries, a bound that some block reaches.
All inputs are finite; a program needn't handle non-finite values.
Results may differ from a plain program's by a relative error of at most 0.014.
Values may be sent and summed in bfloat16 or wider, within the bound.
A program may use at most 64 MiB of HBM per device.

v0:
```python
import jax
import jax.numpy as jnp
from jax import lax
from jax.sharding import PartitionSpec as P


def rms_norm(value, gain):
    return value * lax.rsqrt(jnp.mean(value * value, axis=-1, keepdims=True) + 1e-06) * gain


def rounded_term(value):
    return lax.optimization_barrier(value.astype(jnp.bfloat16)).astype(jnp.float32)


def on_device(
    tokens,
    lru_state,
    conv_window,
    gain_mix_in,
    gain_mix_out,
    gain_ffn_in,
    gain_ffn_out,
    w_branch,
    w_input,
    conv_taps,
    gate_a,
    gate_x,
    decay_rate,
    w_mix_out,
    routes,
    route_weight,
    expert_gate,
    expert_up,
    expert_down,
    shared_gate,
    shared_up,
    shared_down,
):
    resid = tokens.astype(jnp.float32)
    normed = rms_norm(resid, gain_mix_in).astype(jnp.bfloat16)
    branch = jnp.dot(normed, w_branch, preferred_element_type=jnp.float32)
    inflow = jnp.dot(normed, w_input, preferred_element_type=jnp.float32).astype(jnp.bfloat16)
    window = jnp.concatenate([conv_window, inflow[:, None, :]], axis=1)
    new_window = window[:, 1:]
    conv = jnp.sum(window.astype(jnp.float32) * conv_taps.astype(jnp.float32)[None], axis=1)
    count, local_ch = conv.shape
    groups, group_dim = (gate_a.shape[0], gate_a.shape[1])
    grouped = conv.astype(jnp.bfloat16).reshape(count, groups, group_dim)
    recur_gate = jax.nn.sigmoid(
        jnp.einsum("sbi,bij->sbj", grouped, gate_a, preferred_element_type=jnp.float32).reshape(
            count, local_ch
        )
    )
    input_gate = jax.nn.sigmoid(
        jnp.einsum("sbi,bij->sbj", grouped, gate_x, preferred_element_type=jnp.float32).reshape(
            count, local_ch
        )
    )
    log_decay = -8.0 * recur_gate * decay_rate[None]
    new_state = (
        jnp.exp(log_decay) * lru_state + jnp.sqrt(-jnp.expm1(2.0 * log_decay)) * conv * input_gate
    )
    gated = (new_state * jax.nn.gelu(branch)).astype(jnp.bfloat16)
    mix_term = rounded_term(jnp.dot(gated, w_mix_out, preferred_element_type=jnp.float32))
    mixed = lax.psum(mix_term.astype(jnp.bfloat16), "tp").astype(jnp.float32)
    middle = (resid + rms_norm(mixed, gain_mix_out)).astype(jnp.bfloat16)
    ffn_in = rms_norm(middle.astype(jnp.float32), gain_ffn_in).astype(jnp.bfloat16)
    width = ffn_in.shape[1]
    top = routes.shape[1]
    local_exp = expert_gate.shape[0]
    experts = local_exp * lax.axis_size("ep")
    capacity = max(2, 2 * count * top // experts)
    flat = routes.reshape(count * top)
    onehot = (flat[:, None] == jnp.arange(experts, dtype=jnp.int32)[None, :]).astype(jnp.int32)
    rank = jnp.sum(onehot * (jnp.cumsum(onehot, axis=0) - 1), axis=-1)
    dest = flat * capacity + rank
    slot_ids = jnp.arange(experts * capacity, dtype=jnp.int32)
    placed = jnp.any(dest.reshape(count, top)[None, :, :] == slot_ids[:, None, None], axis=-1)
    outbound = jnp.dot(placed.astype(jnp.bfloat16), ffn_in, preferred_element_type=jnp.float32)
    outbound = outbound.astype(jnp.bfloat16).reshape(experts, capacity, width)
    shared_hidden = (
        jax.nn.silu(jnp.dot(ffn_in, shared_gate, preferred_element_type=jnp.float32))
        * jnp.dot(ffn_in, shared_up, preferred_element_type=jnp.float32)
    ).astype(jnp.bfloat16)
    shared = lax.psum(
        rounded_term(
            jnp.dot(shared_hidden, shared_down, preferred_element_type=jnp.float32)
        ).astype(jnp.bfloat16),
        "tp",
    ).astype(jnp.float32)
    share = width // lax.axis_size("tp")
    own = lax.dynamic_slice_in_dim(outbound, lax.axis_index("tp") * share, share, 2)
    arrived = lax.all_to_all(own, "ep", split_axis=0, concat_axis=1, tiled=True)
    rows = lax.all_gather(arrived, "tp", axis=2, tiled=True)
    hidden = (
        jax.nn.silu(
            jnp.einsum("erd,edf->erf", rows, expert_gate, preferred_element_type=jnp.float32)
        )
        * jnp.einsum("erd,edf->erf", rows, expert_up, preferred_element_type=jnp.float32)
    ).astype(jnp.bfloat16)
    summed = lax.psum_scatter(
        rounded_term(
            jnp.einsum("erf,efd->erd", hidden, expert_down, preferred_element_type=jnp.float32)
        ).astype(jnp.bfloat16),
        "tp",
        scatter_dimension=2,
        tiled=True,
    )
    back = lax.all_to_all(summed, "ep", split_axis=1, concat_axis=0, tiled=True)
    flat_out = back.reshape(experts * capacity, share)
    picked = flat_out[dest].reshape(count, top, flat_out.shape[1])
    routed_share = jnp.sum(picked.astype(jnp.float32) * route_weight[:, :, None], axis=1).astype(
        jnp.bfloat16
    )
    routed = lax.all_gather(routed_share, "tp", axis=1, tiled=True)
    total = routed.astype(jnp.float32) + shared
    layer_out = (middle.astype(jnp.float32) + rms_norm(total, gain_ffn_out)).astype(jnp.bfloat16)
    return (layer_out, new_state, new_window)


def solution(mesh):
    placed = (
        P("ep", None),
        P("ep", "tp"),
        P("ep", None, "tp"),
        P(),
        P(),
        P(),
        P(),
        P(None, "tp"),
        P(None, "tp"),
        P(None, "tp"),
        P("tp", None, None),
        P("tp", None, None),
        P("tp"),
        P("tp", None),
        P("ep", None),
        P("ep", None),
        P("ep", None, "tp"),
        P("ep", None, "tp"),
        P("ep", "tp", None),
        P(None, "tp"),
        P(None, "tp"),
        P("tp", None),
    )
    return jax.shard_map(
        on_device,
        mesh=mesh,
        in_specs=placed,
        out_specs=(P("ep", None), P("ep", "tp"), P("ep", None, "tp")),
        check_vma=False,
    )
```

profile of v0, /device:TPU:0, one launch (start us, length us, event | category | flops | bytes accessed | tf_op | source)
XLA Modules:
  0.0 134.1 jit_solution(11292914418998984690)
XLA Ops:
  7.3 1.2 fusion.24
  8.5 0.7 convert_element_type.92
  9.2 2.2 %fusion.10 = bf16[32,1,512]{2,0,1:T(8,128)(2,1)S(1)} fusion(bf16[2048,512]{1,0:T(8,128)(2,1)} %param.30, bf16[32,2048]{1,0:T(8,128)(2,1)} %param.22, f32[2048]{0:T(1024)} %param.25, f32[32]{0:T(128)S(1)} %add_rsqrt_fusion.3), kind=kOutput, calls=%fused_computation.19 | convolution fusion | flops 67387392 | bytes 2269312 | tf_op jit(solution)/shard_map/dot_general | solution.py:42
  11.5 0.2 fusion.5
  11.6 0.2 fusion.9
  11.9 0.1 fusion.49
  12.0 3.2 %convolution_convert_fusion.3 = bf16[32,2048]{1,0:T(8,128)(2,1)} fusion(bf16[512,2048]{1,0:T(8,128)(2,1)S(1)} %copy-done, f32[32,512]{1,0:T(8,128)S(1)} %fusion.49, bf16[2048,512]{1,0:T(8,128)(2,1)} %param.29, bf16[32,2048]{1,0:T(8,128)(2,1)S(1)} %copy-done.2, f32[2048]{0:T(1024)S(1)} %copy-done.10, f32[32]{0:T(128)S(1)} %add_rsqrt_fusion.3), kind=kOutput, calls=%fused_computation.5 | convolution fusion | flops 134709248 | bytes 4530304 | tf_op jit(solution)/shard_map/dot_general | solution.py:64
  15.3 0.0 all-gather.2.cloned.1.call-start
  15.3 0.1 copy.57
  15.4 0.1 eq.28
  15.5 0.1 fusion.50
  15.6 0.2 reduce_window_sum.11
  15.8 0.2 select_reduce_fusion
  16.0 0.1 reduce_sum.71
  16.1 0.6 broadcast_multiply_fusion
  16.7 0.1 copy.59
  16.8 0.1 fusion.38
  16.9 19.2 %all-reduce.3.cloned.1.call-done = bf16[32,2048]{1,0:T(8,128)(2,1)} async-done(((bf16[32,2048]{1,0:T(8,128)(2,1)}), bf16[32,2048]{1,0:T(8,128)(2,1)}) %all-reduce.3.cloned.1.call-update) | async-done | bytes 131088 | tf_op jit(solution)/shard_map/psum | solution.py:65
  36.1 1.0 fusion.22
  37.1 1.1 fusion.28
  38.3 0.5 convolution_convert_fusion.1
  38.9 22.2 %all_to_all.21 = bf16[16,16,1024]{2,1,0:T(8,128)(2,1)} all-to-all(bf16[16,16,1024]{2,1,0:T(8,128)(2,1)S(1)} %constant_dynamic-slice_fusion), channel_id=1, replica_groups=mesh['ep'=16,'tp'=2] {'ep'}, dimensions={0} | all-to-all | bytes 1048576 | tf_op jit(solution)/shard_map/all_to_all | solution.py:93
  61.1 0.0 reduce-scatter.2.cloned.1.call-start
  61.1 7.5 %all-gather.2.cloned.1.call-done = bf16[1,256,2048]{2,1,0:T(8,128)(2,1)} async-done(((bf16[1,256,1024]{2,1,0:T(8,128)(2,1)}), bf16[1,256,2048]{2,1,0:T(8,128)(2,1)}) %all-gather.2.cloned.1.call-update) | async-done | bytes 1048592 | tf_op jit(solution)/shard_map/all_gather | solution.py:94
  68.6 2.1 %fusion.14 = f32[256,256]{1,0:T(8,128)S(1)} fusion(bf16[1,2048,256]{2,1,0:T(8,128)(2,1)} %param.38, bf16[1,256,2048]{2,1,0:T(8,128)(2,1)} %all-gather.2.cloned.1.call-done), kind=kOutput, calls=%fused_computation.24 | convolution fusion | flops 268435456 | bytes 2359296 | tf_op jit(solution)/shard_map/erd,edf->erf/dot_general | solution.py:97
  70.7 3.8 %fusion = bf16[1,256,2048]{2,1,0:T(8,128)(2,1)} fusion(bf16[1,256,2048]{2,1,0:T(8,128)(2,1)} %param.40, bf16[1,2048,256]{2,1,0:T(8,128)(2,1)} %param.39, bf16[1,256,2048]{2,1,0:T(8,128)(2,1)S(1)} %copy-done.1, f32[256,256]{1,0:T(8,128)S(1)} %fusion.14), kind=kOutput, calls=%fused_computation.3 | convolution fusion | flops 537788416 | bytes 4456448 | tf_op jit(solution)/shard_map/erf,efd->erd/dot_general | solution.py:103
  74.6 0.8 mul.225
  75.4 0.8 copy.61
  76.2 8.1 %reduce-scatter.2.cloned.1.call-done = bf16[1,256,1024]{2,1,0:T(8,128)(2,1)} async-done(((bf16[1,256,2048]{2,1,0:T(8,128)(2,1)}), bf16[1,256,1024]{2,1,0:T(8,128)(2,1)}) %reduce-scatter.2.cloned.1.call-update) | async-done | bytes 524304 | tf_op jit(solution)/shard_map/reduce_scatter | solution.py:101
  84.3 1.9 %copy.81 = bf16[1,256,1024]{2,0,1:T(2,128)(2,1)S(1)} copy(bf16[1,256,1024]{2,1,0:T(8,128)(2,1)} %reduce-scatter.2.cloned.1.call-done) | data formatting | bytes 1048576 | tf_op jit(solution)/shard_map/reduce_scatter | solution.py:101
  86.2 0.5 broadcast.143
  86.7 4.5 %reduce = bf16[256,1024]{1,0:T(8,128)(2,1)} reduce(bf16[256,1,1024]{2,1,0:T(2,128)(2,1)S(1)} %bitcast.73, bf16[]{:T(256)} %broadcast.143), dimensions={1}, to_apply=%bitcast.70.reduce_sub_computation | reduce | bytes 1048578
  91.2 2.2 %reshape.155 = bf16[16,2,8192]{2,1,0:T(2,128)(2,1)} reshape(bf16[256,1024]{1,0:T(8,128)(2,1)} %reduce) | data formatting | bytes 1048576
  93.4 6.8 %all-to-all-start.1 = ((bf16[16,2,8192]{2,1,0:T(2,128)(2,1)}), bf16[16,2,8192]{2,1,0:T(2,128)(2,1)S(1)}, u32[]{:S(2)}, u32[]{:S(2)}) async-start(bf16[16,2,8192]{2,1,0:T(2,128)(2,1)} %reshape.155), calls=%async_computation.2 | async-start | bytes 1048576 | tf_op jit(solution)/shard_map/all_to_all | solution.py:109
  100.2 0.0 all-reduce.5.cloned.1.call-start
  100.3 0.7 fusion.39
  100.9 1.5 %fusion.82 = f32[32,256]{1,0:T(8,128)S(1)} fusion(bf16[2048,256]{1,0:T(8,128)(2,1)} %param.41, bf16[32,2048]{1,0:T(8,128)(2,1)S(1)} %get-tuple-element.4, f32[2048]{0:T(1024)S(1)} %copy-done.8, f32[32]{0:T(128)S(1)} %add_rsqrt_fusion.1), kind=kOutput, calls=%fused_computation.113 | convolution fusion | flops 33816576 | bytes 1220736 | tf_op jit(solution)/shard_map/dot_general | solution.py:82
  102.5 3.0 %convolution_convert_fusion.2 = bf16[32,2048]{1,0:T(8,128)(2,1)} fusion(bf16[256,2048]{1,0:T(8,128)(2,1)} %param.43, bf16[2048,256]{1,0:T(8,128)(2,1)} %param.42, f32[32,256]{1,0:T(8,128)S(1)} %fusion.82, bf16[32,2048]{1,0:T(8,128)(2,1)S(1)} %get-tuple-element.4, f32[2048]{0:T(1024)S(1)} %copy-done.8, f32[32]{0:T(128)S(1)} %add_rsqrt_fusion.1), kind=kOutput, calls=%fused_computation.4 | convolution fusion | flops 67485696 | bytes 2400384 | tf_op jit(solution)/shard_map/dot_general | solution.py:87
  105.5 10.2 %all-to-all-done.1 = bf16[16,2,8192]{2,1,0:T(2,128)(2,1)S(1)} async-done(((bf16[16,2,8192]{2,1,0:T(2,128)(2,1)}), bf16[16,2,8192]{2,1,0:T(2,128)(2,1)S(1)}, u32[]{:S(2)}, u32[]{:S(2)}) %all-to-all-start.1) | async-done | bytes 524320 | tf_op jit(solution)/shard_map/all_to_all | solution.py:109
  115.7 1.8 %reshape.156 = bf16[256,1,1024]{2,1,0:T(2,128)(2,1)} reshape(bf16[16,2,8192]{2,1,0:T(2,128)(2,1)S(1)} %all-to-all-done.1) | data formatting | bytes 1048576
  117.4 1.4 %copy.80 = bf16[1,256,1024]{2,1,0:T(8,128)(2,1)S(1)} copy(bf16[1,256,1024]{2,0,1:T(2,128)(2,1)} %bitcast.72) | data formatting | bytes 1048576
  118.9 0.9 gather_fusion
  119.7 0.2 reshape.146
  119.9 0.4 multiply_reduce_fusion
  120.3 1.9 %all_gather.7 = bf16[32,2048]{1,0:T(8,128)(2,1)S(1)} all-gather(bf16[32,1024]{1,0:T(8,128)(2,1)S(1)} %multiply_reduce_fusion), channel_id=1, replica_groups=mesh['ep'=16,'tp'=2] {'tp'}, dimensions={1}, use_global_device_ids=true | all-gather | bytes 196608 | tf_op jit(solution)/shard_map/all_gather | solution.py:115
  122.2 2.7 %all-reduce.5.cloned.1.call-done = bf16[32,2048]{1,0:T(8,128)(2,1)} async-done(((bf16[32,2048]{1,0:T(8,128)(2,1)}), bf16[32,2048]{1,0:T(8,128)(2,1)}) %all-reduce.5.cloned.1.call-update) | async-done | bytes 131088 | tf_op jit(solution)/shard_map/psum | solution.py:85
  124.8 1.1 multiply_reduce_fusion.1
  125.9 1.7 %fusion.31 = bf16[32,2048]{1,0:T(8,128)(2,1)} fusion(bf16[32,2048]{1,0:T(8,128)(2,1)S(1)} %get-tuple-element.4, bf16[32,2048]{1,0:T(8,128)(2,1)} %all-reduce.5.cloned.1.call-done, bf16[32,2048]{1,0:T(8,128)(2,1)S(1)} %all_gather.7, f32[2048]{0:T(1024)S(1)} %copy-done.11, f32[32]{0:T(128)S(1)} %add_rsqrt_fusion), kind=kLoop, calls=%fused_computation.47 | loop fusion | flops 524288 | bytes 532608 | tf_op jit(solution)/shard_map/convert_element_type | solution.py:117
  (48 shorter events, 0.3 us)
Async XLA Ops:
  7.2 4.8 %copy-start = (bf16[512,2048]{1,0:T(8,128)(2,1)S(1)}, bf16[512,2048]{1,0:T(8,128)(2,1)}, u32[]{:S(2)}) copy-start(bf16[512,2048]{1,0:T(8,128)(2,1)} %param.35) | copy-start | bytes 6291460
  7.2 4.8 %copy-start.2 = (bf16[32,2048]{1,0:T(8,128)(2,1)S(1)}, bf16[32,2048]{1,0:T(8,128)(2,1)}, u32[]{:S(2)}) copy-start(bf16[32,2048]{1,0:T(8,128)(2,1)} %param.22) | copy-start | bytes 393220
  7.2 4.8 %copy-start.10 = (f32[2048]{0:T(1024)S(1)}, f32[2048]{0:T(1024)}, u32[]{:S(2)}) copy-start(f32[2048]{0:T(1024)} %param.25) | copy-start | bytes 24580
  7.2 4.2 %copy-start.3 = (bf16[32,3,512]{2,0,1:T(8,128)(2,1)S(1)}, bf16[32,3,512]{2,0,1:T(8,128)(2,1)}, u32[]{:S(2)}) copy-start(bf16[32,3,512]{2,0,1:T(8,128)(2,1)} %param.24) | copy-start | bytes 294916
  7.2 4.2 %copy-start.15 = (bf16[4,128,128]{2,1,0:T(8,128)(2,1)S(1)}, bf16[4,128,128]{2,1,0:T(8,128)(2,1)}, u32[]{:S(2)}) copy-start(bf16[4,128,128]{2,1,0:T(8,128)(2,1)} %param.33) | copy-start | bytes 393220
  7.2 4.4 %copy-start.16 = (bf16[4,128,128]{2,1,0:T(8,128)(2,1)S(1)}, bf16[4,128,128]{2,1,0:T(8,128)(2,1)}, u32[]{:S(2)}) copy-start(bf16[4,128,128]{2,1,0:T(8,128)(2,1)} %param.32) | copy-start | bytes 393220
  7.2 4.6 %copy-start.14 = (f32[512]{0:T(512)S(1)}, f32[512]{0:T(512)}, u32[]{:S(2)}) copy-start(f32[512]{0:T(512)} %param.34) | copy-start | bytes 6148
  7.2 4.6 %copy-start.9 = (f32[32,512]{1,0:T(8,128)S(1)}, f32[32,512]{1,0:T(8,128)}, u32[]{:S(2)}) copy-start(f32[32,512]{1,0:T(8,128)} %param.23) | copy-start | bytes 196612
  7.3 28.8 %all-reduce.3.cloned.1.call-start = ((), (), s32[]{:S(2)}) async-start(), calls=%async_computation.3 | async-start | bytes 262144 | tf_op jit(solution)/shard_map/psum | solution.py:65
  11.4 3.8 %copy-start.5 = (bf16[32,1,512]{2,0,1:T(8,128)(2,1)}, bf16[32,1,512]{2,0,1:T(8,128)(2,1)S(1)}, u32[]{:S(2)}) copy-start(bf16[32,1,512]{2,0,1:T(8,128)(2,1)S(1)} %fusion.10) | copy-start | bytes 98308
  12.0 3.3 %copy-start.7 = (f32[32,512]{1,0:T(8,128)}, f32[32,512]{1,0:T(8,128)S(1)}, u32[]{:S(2)}) copy-start(f32[32,512]{1,0:T(8,128)S(1)} %fusion.49) | copy-start | bytes 196612
  12.0 3.4 %copy-start.13 = (s32[32,4]{0,1:T(4,128)S(1)}, s32[32,4]{0,1:T(4,128)}, u32[]{:S(2)}) copy-start(s32[32,4]{0,1:T(4,128)} %param.36) | copy-start | bytes 1540
  12.0 25.1 %copy-start.12 = (f32[2048]{0:T(1024)S(1)}, f32[2048]{0:T(1024)}, u32[]{:S(2)}) copy-start(f32[2048]{0:T(1024)} %param.26) | copy-start | bytes 24580
  12.0 26.3 %copy-start.8 = (f32[2048]{0:T(1024)S(1)}, f32[2048]{0:T(1024)}, u32[]{:S(2)}) copy-start(f32[2048]{0:T(1024)} %param.27) | copy-start | bytes 24580
  15.3 53.4 %all-gather.2.cloned.1.call-start = ((), (), s32[]{:S(2)}) async-start(), calls=%async_computation.4 | async-start | bytes 1572864 | tf_op jit(solution)/shard_map/all_gather | solution.py:94
  61.1 23.2 %reduce-scatter.2.cloned.1.call-start = ((), (), s32[]{:S(2)}) async-start(), calls=%async_computation.5 | async-start | bytes 1572864 | tf_op jit(solution)/shard_map/reduce_scatter | solution.py:101
  68.6 2.1 %copy-start.1 = (bf16[1,256,2048]{2,1,0:T(8,128)(2,1)S(1)}, bf16[1,256,2048]{2,1,0:T(8,128)(2,1)}, u32[]{:S(2)}) copy-start(bf16[1,256,2048]{2,1,0:T(8,128)(2,1)} %all-gather.2.cloned.1.call-done) | copy-start | bytes 3145732
  86.1 14.1 %copy-start.4 = (bf16[32,3,512]{2,0,1:T(8,128)(2,1)S(1)}, bf16[32,3,512]{2,0,1:T(8,128)(2,1)}, u32[]{:S(2)}) copy-start(bf16[32,3,512]{2,0,1:T(8,128)(2,1)} %param.24) | copy-start | bytes 294916
  86.2 14.1 %copy-start.6 = (bf16[32,1,512]{2,0,1:T(8,128)(2,1)S(1)}, bf16[32,1,512]{2,0,1:T(8,128)(2,1)}, u32[]{:S(2)}) copy-start(bf16[32,1,512]{2,0,1:T(8,128)(2,1)} %copy-done.5) | copy-start | bytes 98308
  93.4 22.3 %all-to-all-start.1 = ((bf16[16,2,8192]{2,1,0:T(2,128)(2,1)}), bf16[16,2,8192]{2,1,0:T(2,128)(2,1)S(1)}, u32[]{:S(2)}, u32[]{:S(2)}) async-start(bf16[16,2,8192]{2,1,0:T(2,128)(2,1)} %reshape.155), calls=%async_computation.2 | async-start | bytes 1048576 | tf_op jit(solution)/shard_map/all_to_all | solution.py:109
  100.2 24.7 %all-reduce.5.cloned.1.call-start = ((), (), s32[]{:S(2)}) async-start(), calls=%async_computation.6 | async-start | bytes 262144 | tf_op jit(solution)/shard_map/psum | solution.py:85
  118.8 7.1 %copy-start.11 = (f32[2048]{0:T(1024)S(1)}, f32[2048]{0:T(1024)}, u32[]{:S(2)}) copy-start(f32[2048]{0:T(1024)} %param.28) | copy-start | bytes 24580
Sparse Core Ops, SparseCore 0:
  15.4 20.6 all-reduce.2
  61.2 7.3 all-gather.1
  74.7 9.5 reduce-scatter.1
  105.6 19.1 all-reduce.4
where the time goes:
time: 135 us; the launch traced here: 134 us
  waiting for transfers between devices  47.7 us (35%)
  blocking collectives  24.1 us (18%)
  matrix products  16.7 us (12%)
  between operations  14.2 us (11%)
  other arithmetic  13.6 us (10%)
  local copies, waits for them, and re-layouts  10.9 us (8%)
  starting transfers between devices  6.93 us (5%)
    all_to_all x1, blocking collectives, on_device(): arrived = lax.all_to_all(own, 'ep', split_axis=0, concat_axis=1, tiled=True)  22.2 us
    psum x1, waiting for transfers between devices, on_device(): mixed = lax.psum(mix_term.astype(jnp.bfloat16), 'tp').astype(jnp.float32)  19.2 us
    all_to_all x1, waiting for transfers between devices, on_device(): back = lax.all_to_all(summed, 'ep', split_axis=1, concat_axis=0, tiled=True)  10.2 us
    reduce_scatter x1, waiting for transfers between devices, on_device(): lax.psum_scatter(rounded_term(jnp.einsum('erf,efd->erd', hidden, expert_d...  8.14 us
    all_gather x1, waiting for transfers between devices, on_device(): rows = lax.all_gather(arrived, 'tp', axis=2, tiled=True)  7.49 us
    unnamed x40, local copies, waits for them, and re-layouts  6.86 us
    all_to_all x1, starting transfers between devices, on_device(): back = lax.all_to_all(summed, 'ep', split_axis=1, concat_axis=0, tiled=True)  6.77 us
    unnamed x1, other arithmetic  4.5 us
  transfers between devices with their start and end apart: 5, of which 5 were waited for; matrix products, arithmetic and copies ran while one was open for 10% of the time, Pallas kernels for 0%

commit v1 on v0

--- a/solution.py
+++ b/solution.py
@@ -1,7 +1,20 @@
+import functools
 import jax
 import jax.numpy as jnp
 from jax import lax
 from jax.sharding import PartitionSpec as P
+
+
+def follow_arrays_on(in_array, mesh_ax):
+    return jnp.concatenate(
+        jax.lax.all_to_all(
+            jnp.stack(jnp.split(in_array, jax.lax.psum(1, mesh_ax), axis=1), axis=0), mesh_ax, 0, 0
+        ),
+        axis=0,
+    )
+
+
+do_the_case = functools.partial(follow_arrays_on, mesh_ax="ep")
 
 
 def rms_norm(value, gain):
@@ -106,7 +119,7 @@
         scatter_dimension=2,
         tiled=True,
     )
-    back = lax.all_to_all(summed, "ep", split_axis=1, concat_axis=0, tiled=True)
+    back = do_the_case(summed)
     flat_out = back.reshape(experts * capacity, share)
     picked = flat_out[dest].reshape(count, top, flat_out.shape[1])
     routed_share = jnp.sum(picked.astype(jnp.float32) * route_weight[:, :, None], axis=1).astype(

time: 135 us -> 149 us (1.10)
  local copies, waits for them, and re-layouts: 10.9 us -> 24.9 us
  other arithmetic: 13.6 us -> 9.12 us
  waiting for transfers between devices: 47.7 us -> 50.9 us
    unnamed x40 -> x51, local copies, waits for them, and re-layouts: 6.86 us -> 21.4 us
    unnamed x1 -> x0, other arithmetic: 4.5 us -> none
    psum x1, waiting for transfers between devices: 2.65 us -> 5.84 us  [on_device(): lax.psum(rounded_term(jnp.dot(shared_hidden, shared_down, preferred_eleme...]
    reduce_scatter x1 -> x0, local copies, waits for them, and re-layouts: 1.85 us -> none  [on_device(): lax.psum_scatter(rounded_term(jnp.einsum('erf,efd->erd', hidden, expert_d...]
  transfers between devices with their start and end apart: 5 -> 5, of which waited for: 5 -> 5; matrix products, arithmetic and copies ran while one was open for 10% -> 7% of each run, Pallas kernels for 0% -> 0%
where the time goes in v1:
time: 149 us; the launch traced here: 147 us
  waiting for transfers between devices  50.9 us (34%)
  local copies, waits for them, and re-layouts  24.9 us (17%)
  blocking collectives  24.1 us (16%)
  matrix products  16.7 us (11%)
  between operations  14.1 us (9%)
  other arithmetic  9.12 us (6%)
  starting transfers between devices  6.93 us (5%)
    all_to_all x1, blocking collectives, on_device(): arrived = lax.all_to_all(own, 'ep', split_axis=0, concat_axis=1, tiled=True)  22.2 us
    unnamed x51, local copies, waits for them, and re-layouts  21.4 us
    psum x1, waiting for transfers between devices, on_device(): mixed = lax.psum(mix_term.astype(jnp.bfloat16), 'tp').astype(jnp.float32)  19.2 us
    all_to_all x1, waiting for transfers between devices, follow_arrays_on(): jax.lax.all_to_all(jnp.stack(jnp.split(in_array, jax.lax.psum(1, mesh_ax)...  10.2 us
    reduce_scatter x1, waiting for transfers between devices, on_device(): lax.psum_scatter(rounded_term(jnp.einsum('erf,efd->erd', hidden, expert_d...  8.11 us
    all_gather x1, waiting for transfers between devices, on_device(): rows = lax.all_gather(arrived, 'tp', axis=2, tiled=True)  7.49 us
    all_to_all x1, starting transfers between devices, follow_arrays_on(): jax.lax.all_to_all(jnp.stack(jnp.split(in_array, jax.lax.psum(1, mesh_ax)...  6.77 us
    psum x1, waiting for transfers between devices, on_device(): lax.psum(rounded_term(jnp.dot(shared_hidden, shared_down, preferred_eleme...  5.84 us
  transfers between devices with their start and end apart: 5, of which 5 were waited for; matrix products, arithmetic and copies ran while one was open for 7% of the time, Pallas kernels for 0%

profile of v1, /device:TPU:0, one launch (start us, length us, event | category | flops | bytes accessed | tf_op | source)
XLA Modules:
  0.0 146.8 jit_solution(12892355222082966497)
XLA Ops:
  7.3 1.2 fusion.24
  8.5 0.7 convert_element_type.92
  9.2 2.2 %fusion.10 = bf16[32,1,512]{2,0,1:T(8,128)(2,1)S(1)} fusion(bf16[2048,512]{1,0:T(8,128)(2,1)} %param.30, bf16[32,2048]{1,0:T(8,128)(2,1)} %param.22, f32[2048]{0:T(1024)} %param.25, f32[32]{0:T(128)S(1)} %add_rsqrt_fusion.3), kind=kOutput, calls=%fused_computation.19 | convolution fusion | flops 67387392 | bytes 2269312 | tf_op jit(solution)/shard_map/dot_general | solution.py:55
  11.5 0.2 fusion.5
  11.6 0.2 fusion.9
  12.0 3.2 %convolution_convert_fusion.3 = bf16[32,2048]{1,0:T(8,128)(2,1)} fusion(bf16[512,2048]{1,0:T(8,128)(2,1)S(1)} %copy-done, f32[32,512]{1,0:T(8,128)S(1)} %fusion.49, bf16[2048,512]{1,0:T(8,128)(2,1)} %param.29, bf16[32,2048]{1,0:T(8,128)(2,1)S(1)} %copy-done.2, f32[2048]{0:T(1024)S(1)} %copy-done.10, f32[32]{0:T(128)S(1)} %add_rsqrt_fusion.3), kind=kOutput, calls=%fused_computation.5 | convolution fusion | flops 134709248 | bytes 4530304 | tf_op jit(solution)/shard_map/dot_general | solution.py:77
  15.6 0.2 reduce_window_sum.11
  15.8 0.2 select_reduce_fusion
  16.1 0.6 broadcast_multiply_fusion
  16.9 19.2 %all-reduce.3.cloned.1.call-done = bf16[32,2048]{1,0:T(8,128)(2,1)} async-done(((bf16[32,2048]{1,0:T(8,128)(2,1)}), bf16[32,2048]{1,0:T(8,128)(2,1)}) %all-reduce.3.cloned.1.call-update) | async-done | bytes 131088 | tf_op jit(solution)/shard_map/psum | solution.py:78
  36.1 1.0 fusion.22
  37.1 1.1 fusion.28
  38.3 0.5 convolution_convert_fusion.1
  38.9 22.2 %all_to_all.17 = bf16[16,16,1024]{2,1,0:T(8,128)(2,1)} all-to-all(bf16[16,16,1024]{2,1,0:T(8,128)(2,1)S(1)} %constant_dynamic-slice_fusion), channel_id=1, replica_groups=mesh['ep'=16,'tp'=2] {'ep'}, dimensions={0} | all-to-all | bytes 1048576 | tf_op jit(solution)/shard_map/all_to_all | solution.py:106
  61.1 7.5 %all-gather.2.cloned.1.call-done = bf16[1,256,2048]{2,1,0:T(8,128)(2,1)} async-done(((bf16[1,256,1024]{2,1,0:T(8,128)(2,1)}), bf16[1,256,2048]{2,1,0:T(8,128)(2,1)}) %all-gather.2.cloned.1.call-update) | async-done | bytes 1048592 | tf_op jit(solution)/shard_map/all_gather | solution.py:107
  68.6 2.1 %fusion.14 = f32[256,256]{1,0:T(8,128)S(1)} fusion(bf16[1,2048,256]{2,1,0:T(8,128)(2,1)} %param.38, bf16[1,256,2048]{2,1,0:T(8,128)(2,1)} %all-gather.2.cloned.1.call-done), kind=kOutput, calls=%fused_computation.24 | convolution fusion | flops 268435456 | bytes 2359296 | tf_op jit(solution)/shard_map/erd,edf->erf/dot_general | solution.py:110
  70.7 3.8 %fusion = bf16[1,256,2048]{2,1,0:T(8,128)(2,1)} fusion(bf16[1,256,2048]{2,1,0:T(8,128)(2,1)} %param.40, bf16[1,2048,256]{2,1,0:T(8,128)(2,1)} %param.39, bf16[1,256,2048]{2,1,0:T(8,128)(2,1)S(1)} %copy-done.1, f32[256,256]{1,0:T(8,128)S(1)} %fusion.14), kind=kOutput, calls=%fused_computation.3 | convolution fusion | flops 537788416 | bytes 4456448 | tf_op jit(solution)/shard_map/erf,efd->erd/dot_general | solution.py:116
  74.6 0.9 mul.225
  75.4 0.8 copy.44
  76.2 8.1 %reduce-scatter.2.cloned.1.call-done = bf16[1,256,1024]{2,1,0:T(8,128)(2,1)} async-done(((bf16[1,256,2048]{2,1,0:T(8,128)(2,1)}), bf16[1,256,1024]{2,1,0:T(8,128)(2,1)}) %reduce-scatter.2.cloned.1.call-update) | async-done | bytes 524304 | tf_op jit(solution)/shard_map/reduce_scatter | solution.py:114
  84.3 1.4 fusion.75
  85.7 1.4 fusion.74
  87.0 1.4 fusion.73
  88.4 1.4 fusion.72
  89.7 1.4 fusion.71
  91.1 1.4 fusion.70
  92.5 1.4 fusion.69
  93.8 1.4 fusion.68
  95.2 1.4 fusion.67
  96.6 1.4 fusion.66
  97.9 1.4 fusion.65
  99.3 1.4 fusion.64
  100.6 1.4 fusion.63
  102.0 1.4 fusion.62
  103.4 1.4 fusion.61
  104.7 1.4 fusion.60
  106.1 6.8 %all-to-all-start.1 = ((bf16[16,1,16,1024]{3,2,1,0:T(8,128)(2,1)}), bf16[16,1,16,1024]{3,2,1,0:T(8,128)(2,1)S(1)}, u32[]{:S(2)}, u32[]{:S(2)}) async-start(bf16[16,1,16,1024]{3,2,1,0:T(8,128)(2,1)} %fusion.60), calls=%async_computation.2 | async-start | bytes 1048576 | tf_op jit(solution)/shard_map/all_to_all | solution.py:10
  113.0 0.7 fusion.39
  113.6 1.5 %fusion.98 = f32[32,256]{1,0:T(8,128)S(1)} fusion(bf16[2048,256]{1,0:T(8,128)(2,1)} %param.41, bf16[32,2048]{1,0:T(8,128)(2,1)S(1)} %get-tuple-element.4, f32[2048]{0:T(1024)S(1)} %copy-done.8, f32[32]{0:T(128)S(1)} %add_rsqrt_fusion.1), kind=kOutput, calls=%fused_computation.144 | convolution fusion | flops 33816576 | bytes 1220736 | tf_op jit(solution)/shard_map/dot_general | solution.py:95
  115.2 3.0 %convolution_convert_fusion.2 = bf16[32,2048]{1,0:T(8,128)(2,1)} fusion(bf16[256,2048]{1,0:T(8,128)(2,1)} %param.43, bf16[2048,256]{1,0:T(8,128)(2,1)} %param.42, f32[32,256]{1,0:T(8,128)S(1)} %fusion.98, bf16[32,2048]{1,0:T(8,128)(2,1)S(1)} %get-tuple-element.4, f32[2048]{0:T(1024)S(1)} %copy-done.8, f32[32]{0:T(128)S(1)} %add_rsqrt_fusion.1), kind=kOutput, calls=%fused_computation.4 | convolution fusion | flops 67485696 | bytes 2400384 | tf_op jit(solution)/shard_map/dot_general | solution.py:100
  118.2 10.2 %all-to-all-done.1 = bf16[16,1,16,1024]{3,2,1,0:T(8,128)(2,1)S(1)} async-done(((bf16[16,1,16,1024]{3,2,1,0:T(8,128)(2,1)}), bf16[16,1,16,1024]{3,2,1,0:T(8,128)(2,1)S(1)}, u32[]{:S(2)}, u32[]{:S(2)}) %all-to-all-start.1) | async-done | bytes 524320 | tf_op jit(solution)/shard_map/all_to_all | solution.py:10
  128.4 0.9 gather_fusion
  129.2 0.2 reshape.138
  129.4 0.4 multiply_reduce_fusion
  129.8 1.9 %all_gather.7 = bf16[32,2048]{1,0:T(8,128)(2,1)S(1)} all-gather(bf16[32,1024]{1,0:T(8,128)(2,1)S(1)} %multiply_reduce_fusion), channel_id=1, replica_groups=mesh['ep'=16,'tp'=2] {'tp'}, dimensions={1}, use_global_device_ids=true | all-gather | bytes 196608 | tf_op jit(solution)/shard_map/all_gather | solution.py:128
  131.7 5.8 %all-reduce.5.cloned.1.call-done = bf16[32,2048]{1,0:T(8,128)(2,1)} async-done(((bf16[32,2048]{1,0:T(8,128)(2,1)}), bf16[32,2048]{1,0:T(8,128)(2,1)}) %all-reduce.5.cloned.1.call-update) | async-done | bytes 131088 | tf_op jit(solution)/shard_map/psum | solution.py:98
  137.5 1.1 multiply_reduce_fusion.1
  138.6 1.7 %fusion.31 = bf16[32,2048]{1,0:T(8,128)(2,1)} fusion(bf16[32,2048]{1,0:T(8,128)(2,1)S(1)} %get-tuple-element.4, bf16[32,2048]{1,0:T(8,128)(2,1)} %all-reduce.5.cloned.1.call-done, bf16[32,2048]{1,0:T(8,128)(2,1)S(1)} %all_gather.7, f32[2048]{0:T(1024)S(1)} %copy-done.11, f32[32]{0:T(128)S(1)} %add_rsqrt_fusion), kind=kLoop, calls=%fused_computation.46 | loop fusion | flops 524288 | bytes 532608 | tf_op jit(solution)/shard_map/convert_element_type | solution.py:130
  (58 shorter events, 1.1 us)
Async XLA Ops:
  7.2 4.8 %copy-start = (bf16[512,2048]{1,0:T(8,128)(2,1)S(1)}, bf16[512,2048]{1,0:T(8,128)(2,1)}, u32[]{:S(2)}) copy-start(bf16[512,2048]{1,0:T(8,128)(2,1)} %param.35) | copy-start | bytes 6291460
  7.2 4.8 %copy-start.2 = (bf16[32,2048]{1,0:T(8,128)(2,1)S(1)}, bf16[32,2048]{1,0:T(8,128)(2,1)}, u32[]{:S(2)}) copy-start(bf16[32,2048]{1,0:T(8,128)(2,1)} %param.22) | copy-start | bytes 393220
  7.2 4.8 %copy-start.10 = (f32[2048]{0:T(1024)S(1)}, f32[2048]{0:T(1024)}, u32[]{:S(2)}) copy-start(f32[2048]{0:T(1024)} %param.25) | copy-start | bytes 24580
  7.2 4.2 %copy-start.3 = (bf16[32,3,512]{2,0,1:T(8,128)(2,1)S(1)}, bf16[32,3,512]{2,0,1:T(8,128)(2,1)}, u32[]{:S(2)}) copy-start(bf16[32,3,512]{2,0,1:T(8,128)(2,1)} %param.24) | copy-start | bytes 294916
  7.2 4.2 %copy-start.15 = (bf16[4,128,128]{2,1,0:T(8,128)(2,1)S(1)}, bf16[4,128,128]{2,1,0:T(8,128)(2,1)}, u32[]{:S(2)}) copy-start(bf16[4,128,128]{2,1,0:T(8,128)(2,1)} %param.33) | copy-start | bytes 393220
  7.2 4.4 %copy-start.16 = (bf16[4,128,128]{2,1,0:T(8,128)(2,1)S(1)}, bf16[4,128,128]{2,1,0:T(8,128)(2,1)}, u32[]{:S(2)}) copy-start(bf16[4,128,128]{2,1,0:T(8,128)(2,1)} %param.32) | copy-start | bytes 393220
  7.2 4.6 %copy-start.14 = (f32[512]{0:T(512)S(1)}, f32[512]{0:T(512)}, u32[]{:S(2)}) copy-start(f32[512]{0:T(512)} %param.34) | copy-start | bytes 6148
  7.2 4.6 %copy-start.9 = (f32[32,512]{1,0:T(8,128)S(1)}, f32[32,512]{1,0:T(8,128)}, u32[]{:S(2)}) copy-start(f32[32,512]{1,0:T(8,128)} %param.23) | copy-start | bytes 196612
  7.3 28.8 %all-reduce.3.cloned.1.call-start = ((), (), s32[]{:S(2)}) async-start(), calls=%async_computation.3 | async-start | bytes 262144 | tf_op jit(solution)/shard_map/psum | solution.py:78
  11.4 3.8 %copy-start.5 = (bf16[32,1,512]{2,0,1:T(8,128)(2,1)}, bf16[32,1,512]{2,0,1:T(8,128)(2,1)S(1)}, u32[]{:S(2)}) copy-start(bf16[32,1,512]{2,0,1:T(8,128)(2,1)S(1)} %fusion.10) | copy-start | bytes 98308
  12.0 3.3 %copy-start.7 = (f32[32,512]{1,0:T(8,128)}, f32[32,512]{1,0:T(8,128)S(1)}, u32[]{:S(2)}) copy-start(f32[32,512]{1,0:T(8,128)S(1)} %fusion.49) | copy-start | bytes 196612
  12.0 3.4 %copy-start.13 = (s32[32,4]{0,1:T(4,128)S(1)}, s32[32,4]{0,1:T(4,128)}, u32[]{:S(2)}) copy-start(s32[32,4]{0,1:T(4,128)} %param.36) | copy-start | bytes 1540
  12.0 25.1 %copy-start.12 = (f32[2048]{0:T(1024)S(1)}, f32[2048]{0:T(1024)}, u32[]{:S(2)}) copy-start(f32[2048]{0:T(1024)} %param.26) | copy-start | bytes 24580
  12.0 26.3 %copy-start.8 = (f32[2048]{0:T(1024)S(1)}, f32[2048]{0:T(1024)}, u32[]{:S(2)}) copy-start(f32[2048]{0:T(1024)} %param.27) | copy-start | bytes 24580
  15.3 53.4 %all-gather.2.cloned.1.call-start = ((), (), s32[]{:S(2)}) async-start(), calls=%async_computation.4 | async-start | bytes 1572864 | tf_op jit(solution)/shard_map/all_gather | solution.py:107
  61.1 23.2 %reduce-scatter.2.cloned.1.call-start = ((), (), s32[]{:S(2)}) async-start(), calls=%async_computation.5 | async-start | bytes 1572864 | tf_op jit(solution)/shard_map/reduce_scatter | solution.py:114
  68.6 2.1 %copy-start.1 = (bf16[1,256,2048]{2,1,0:T(8,128)(2,1)S(1)}, bf16[1,256,2048]{2,1,0:T(8,128)(2,1)}, u32[]{:S(2)}) copy-start(bf16[1,256,2048]{2,1,0:T(8,128)(2,1)} %all-gather.2.cloned.1.call-done) | copy-start | bytes 3145732
  74.5 38.4 %copy-start.4 = (bf16[32,3,512]{2,0,1:T(8,128)(2,1)S(1)}, bf16[32,3,512]{2,0,1:T(8,128)(2,1)}, u32[]{:S(2)}) copy-start(bf16[32,3,512]{2,0,1:T(8,128)(2,1)} %param.24) | copy-start | bytes 294916
  74.5 38.4 %copy-start.6 = (bf16[32,1,512]{2,0,1:T(8,128)(2,1)S(1)}, bf16[32,1,512]{2,0,1:T(8,128)(2,1)}, u32[]{:S(2)}) copy-start(bf16[32,1,512]{2,0,1:T(8,128)(2,1)} %copy-done.5) | copy-start | bytes 98308
  106.1 22.3 %all-to-all-start.1 = ((bf16[16,1,16,1024]{3,2,1,0:T(8,128)(2,1)}), bf16[16,1,16,1024]{3,2,1,0:T(8,128)(2,1)S(1)}, u32[]{:S(2)}, u32[]{:S(2)}) async-start(bf16[16,1,16,1024]{3,2,1,0:T(8,128)(2,1)} %fusion.60), calls=%async_computation.2 | async-start | bytes 1048576 | tf_op jit(solution)/shard_map/all_to_all | solution.py:10
  112.9 24.7 %all-reduce.5.cloned.1.call-start = ((), (), s32[]{:S(2)}) async-start(), calls=%async_computation.6 | async-start | bytes 262144 | tf_op jit(solution)/shard_map/psum | solution.py:98
  128.3 10.2 %copy-start.11 = (f32[2048]{0:T(1024)S(1)}, f32[2048]{0:T(1024)}, u32[]{:S(2)}) copy-start(f32[2048]{0:T(1024)} %param.28) | copy-start | bytes 24580
Sparse Core Ops, SparseCore 0:
  15.4 20.6 all-reduce.2
  61.2 7.3 all-gather.1
  74.7 9.5 reduce-scatter.1
  118.3 19.1 all-reduce.4
